TPU v7x, 32 devices: a whole 2x2x4 slice. The times are simulated.
32 devices in a mesh: ep: 16 (over z, x, core), tp: 2 (over y).
Axes of the slice: x: 2, y: 2, z: 4, core: 2. Of those that a mesh axis runs over, the one named last changes fastest.
Arguments:
- tokens: bfloat16 [256, 1024], P('ep'), may hold values from -6 to 6
- old_state: float32 [256, 4, 128, 128], P('ep', 'tp'), may hold values from -6 to 6
- query_weight: bfloat16 [1024, 512], P(None, 'tp'), may hold values from -0.1875 to 0.1875
- forget_weight: bfloat16 [1024, 512], P(None, 'tp'), may hold values from -0.1875 to 0.1875
- input_weight: bfloat16 [1024, 512], P(None, 'tp'), may hold values from -0.1875 to 0.1875
- lower_bound: float32 [512], P('tp'), may hold values from 0 to 0.9
- head_gain: float32 [4, 128], P('tp'), may hold values from 0.1 to 1.9
- out_weight: bfloat16 [512, 1024], P('tp'), may hold values from -0.25 to 0.25
- mix_gain: float32 [1024], replicated, may hold values from 0.1 to 1.9
- ffn_gain: float32 [1024], replicated, may hold values from 0.1 to 1.9
- group_weight: bfloat16 [1024, 4], replicated, may hold values from -0.1875 to 0.1875
- expert_weight: bfloat16 [1024, 16], replicated, may hold values from -0.1875 to 0.1875
- routes: int32 [256, 6], P('ep'), may hold values from 0 to 15, all different within a row; in each aligned block of 16 rows (0 to 15, 16 to 31, ...) at most 12 rows name the same one
- gate_weight: bfloat16 [16, 1024, 1024], P('ep', None, 'tp'), may hold values from -0.1875 to 0.1875
- up_weight: bfloat16 [16, 1024, 1024], P('ep', None, 'tp'), may hold values from -0.1875 to 0.1875
- down_weight: bfloat16 [16, 1024, 1024], P('ep', None, 'tp'), may hold values from -0.1875 to 0.1875
Outputs:
- layer_out: bfloat16 [256, 1024], P('ep', 'tp')
- new_state: float32 [256, 4, 128, 128], P('ep', 'tp')
Inputs may be any that keep to these rules, and one draw needn't show every extreme that they name: `routes`: each row names 6 different experts. In each aligned block of 16 rows (the rows of one device) no expert is named more than 12 times, a bound that some block reaches.
All inputs are finite; a program needn't handle non-finite values.
Results may differ from a plain program's by a relative error of at most 0.011.
Values may be sent and summed in bfloat16 or wider, within the bound.
A program may use at most 64 MiB of HBM per device.

v0:
```python
import jax
import jax.numpy as jnp
from jax import lax
from jax.sharding import PartitionSpec as P

epsilon = 1e-06


def scaled_rms(values, gain):
    return values * lax.rsqrt(jnp.mean(values * values, axis=-1, keepdims=True) + epsilon) * gain


def local(
    tokens,
    old_state,
    query_weight,
    forget_weight,
    input_weight,
    lower_bound,
    head_gain,
    out_weight,
    mix_gain,
    ffn_gain,
    group_weight,
    expert_weight,
    routes,
    gate_weight,
    up_weight,
    down_weight,
):
    seq_count, model_width = tokens.shape
    heads_local, head_size = (old_state.shape[1], old_state.shape[2])
    tp_size = lax.axis_size("tp")
    tp_rank = lax.axis_index("tp")
    part_width = model_width // tp_size
    resident = tokens.astype(jnp.float32)
    normed = scaled_rms(resident, mix_gain).astype(jnp.bfloat16)
    query_pre = jnp.dot(normed, query_weight, preferred_element_type=jnp.float32)
    forget_pre = jnp.dot(normed, forget_weight, preferred_element_type=jnp.float32)
    input_pre = jnp.dot(normed, input_weight, preferred_element_type=jnp.float32)
    query = jax.nn.silu(query_pre).reshape(seq_count, heads_local, head_size)
    forget = (lower_bound + (1.0 - lower_bound) * jax.nn.sigmoid(forget_pre)).reshape(
        seq_count, heads_local, head_size
    )
    value = input_pre.reshape(seq_count, heads_local, head_size)
    new_state = forget[..., None] * old_state + (1.0 - forget)[..., None] * value[:, :, None, :]
    readout = jnp.sum(new_state * query[..., None], axis=2)
    head_out = (
        scaled_rms(readout, head_gain)
        .astype(jnp.bfloat16)
        .reshape(seq_count, heads_local * head_size)
    )
    head_part = jnp.dot(head_out, out_weight, preferred_element_type=jnp.float32)
    mixed = lax.psum(head_part.astype(jnp.bfloat16), "tp")
    residual = (resident + mixed.astype(jnp.float32)).astype(jnp.bfloat16)
    ffn_in = scaled_rms(residual.astype(jnp.float32), ffn_gain).astype(jnp.bfloat16)
    experts = expert_weight.shape[1]
    groups = group_weight.shape[1]
    top_count = routes.shape[1]
    group_raw = jnp.exp(jnp.dot(ffn_in, group_weight, preferred_element_type=jnp.float32))
    group_prob = group_raw / jnp.sum(group_raw, axis=-1, keepdims=True)
    expert_raw = jnp.exp(
        jnp.dot(ffn_in, expert_weight, preferred_element_type=jnp.float32)
    ).reshape(seq_count, groups, experts // groups)
    expert_prob = (
        expert_raw / jnp.sum(expert_raw, axis=-1, keepdims=True) * group_prob[:, :, None]
    ).reshape(seq_count, experts)
    expert_ids = jnp.arange(experts, dtype=jnp.int32)
    chosen = routes[:, :, None] == expert_ids[None, None, :]
    weight = jnp.sum(jnp.where(chosen, expert_prob[:, None, :], 0.0), axis=-1)
    gate = weight / jnp.sum(weight, axis=-1, keepdims=True)
    capacity = min(seq_count, max(2, 2 * seq_count * top_count // experts))
    flat = routes.reshape(-1)
    hits = (flat[:, None] == expert_ids[None, :]).astype(jnp.int32)
    before = jnp.cumsum(hits, axis=0) - hits
    slots = jnp.sum(hits * before, axis=1)
    target = flat * capacity + slots
    slot_ids = jnp.arange(experts * capacity, dtype=jnp.int32)
    spread = jnp.sum(
        (slot_ids[:, None, None] == target.reshape(seq_count, top_count)[None, :, :]).astype(
            jnp.int32
        ),
        axis=2,
    ).astype(jnp.bfloat16)
    choose = (target[:, None] == slot_ids[None, :]).astype(jnp.bfloat16)
    outgoing = (
        jnp.dot(spread, ffn_in, preferred_element_type=jnp.float32)
        .astype(jnp.bfloat16)
        .reshape(experts, capacity, model_width)
    )
    arrived = lax.all_to_all(outgoing, "ep", split_axis=0, concat_axis=1, tiled=True)
    gate_hidden = jnp.einsum(
        "erd,edf->erf", arrived, gate_weight, preferred_element_type=jnp.float32
    )
    up_hidden = jnp.einsum("erd,edf->erf", arrived, up_weight, preferred_element_type=jnp.float32)
    hidden = (jax.nn.silu(gate_hidden) * up_hidden).astype(jnp.bfloat16)
    produced = jnp.einsum(
        "erf,efd->erd",
        lax.all_gather(hidden, "tp", axis=2, tiled=True),
        down_weight,
        preferred_element_type=jnp.float32,
    ).astype(jnp.bfloat16)
    returned = lax.all_to_all(produced, "ep", split_axis=1, concat_axis=0, tiled=True)
    picked = jnp.dot(
        choose, returned.reshape(experts * capacity, part_width), preferred_element_type=jnp.float32
    ).reshape(seq_count, top_count, part_width)
    mixture = jnp.sum(gate[:, :, None] * picked, axis=1)
    own_resid = lax.dynamic_slice_in_dim(residual, tp_rank * part_width, part_width, 1).astype(
        jnp.float32
    )
    layer_out = (own_resid + mixture).astype(jnp.bfloat16)
    return (layer_out, new_state)


def solution(mesh):
    in_specs = (
        P("ep", None),
        P("ep", "tp", None, None),
        P(None, "tp"),
        P(None, "tp"),
        P(None, "tp"),
        P("tp"),
        P("tp", None),
        P("tp", None),
        P(),
        P(),
        P(),
        P(),
        P("ep", None),
        P("ep", None, "tp"),
        P("ep", None, "tp"),
        P("ep", None, "tp"),
    )
    out_specs = (P("ep", "tp"), P("ep", "tp", None, None))
    return jax.shard_map(local, mesh=mesh, in_specs=in_specs, out_specs=out_specs, check_vma=False)
```

profile of v0, /device:TPU:0, one launch (start us, length us, event | category | flops | bytes accessed | tf_op | source)
XLA Modules:
  0.0 71.4 jit_solution(7429910828382578727)
XLA Ops:
  0.6 0.0 copy-start
  0.6 0.0 copy-start.1
  0.7 0.9 %copy.77 = s32[16,6]{1,0:T(8,128)S(1)} copy(s32[16,6]{0,1:T(8,128)} %param.28) | data formatting | bytes 768 | tf_op args[12]
  1.6 0.1 eq.73
  1.7 0.1 fusion.25
  1.8 0.1 reduce_window_sum.11
  1.9 0.2 select_reduce_fusion.2
  2.1 0.1 reduce_sum.110
  2.1 0.1 copy.78
  2.2 0.7 multiply_add_fusion.1
  2.9 0.1 convert_reduce_fusion
  3.0 0.9 %fusion.20 = f32[16]{0:T(128)S(1)} fusion(bf16[16,1024]{1,0:T(8,128)(2,1)} %param.16), kind=kLoop, calls=%fused_computation.37 | loop fusion | flops 49136 | bytes 32832 | tf_op jit(solution)/shard_map/reduce_sum | solution.py:10
  3.9 1.3 %divide_multiply_fusion = f32[16,256]{1,0:T(8,128)S(1)} fusion(bf16[1024,256]{1,0:T(8,128)(2,1)} %param.18, bf16[16,1024]{1,0:T(8,128)(2,1)} %param.16, f32[1024]{0:T(1024)} %param.24, f32[16]{0:T(128)S(1)} %add_rsqrt_fusion.2), kind=kOutput, calls=%fused_computation.53 | convolution fusion | flops 8470528 | bytes 577600 | tf_op jit(solution)/shard_map/dot_general | solution.py:38
  5.3 1.3 %fusion.33 = f32[16,256]{1,0:T(8,128)S(1)} fusion(bf16[1024,256]{1,0:T(8,128)(2,1)} %param.20, bf16[16,1024]{1,0:T(8,128)(2,1)} %param.16, f32[1024]{0:T(1024)} %param.24, f32[16]{0:T(128)S(1)} %add_rsqrt_fusion.2), kind=kOutput, calls=%fused_computation.67 | convolution fusion | flops 8454144 | bytes 577600 | tf_op jit(solution)/shard_map/dot_general | solution.py:40
  6.6 0.7 broadcast_subtract_fusion.1
  7.3 1.3 %fusion.8 = f32[16,256]{1,0:T(8,128)S(1)} fusion(bf16[1024,256]{1,0:T(8,128)(2,1)} %param.19, f32[256]{0:T(256)S(1)} %broadcast_subtract_fusion.1, f32[256]{0:T(256)} %param.21, bf16[16,1024]{1,0:T(8,128)(2,1)} %param.16, f32[1024]{0:T(1024)} %param.24, f32[16]{0:T(128)S(1)} %add_rsqrt_fusion.2), kind=kOutput, calls=%fused_computation.16 | convolution fusion | flops 8474624 | bytes 579648 | tf_op jit(solution)/shard_map/dot_general | solution.py:39
  8.6 0.0 copy-done.1
  8.6 0.0 copy-start.6
  8.6 0.0 copy-start.3
  8.7 0.0 copy-start.5
  8.7 3.0 %multiply_reduce_fusion = (f32[16,2,128]{2,1,0:T(2,128)S(1)}, f32[16,2,128,128]{3,2,1,0:T(8,128)}) fusion(f32[16,2,128]{2,1,0:T(2,128)S(1)} %mul.173, f32[16,2,128]{2,1,0:T(2,128)S(1)} %mul.169, f32[16,2,128]{2,1,0:T(2,128)S(1)} %broadcast_subtract_fusion, f32[16,2,128,128]{3,2,1,0:T(8,128)S(1)} %copy-done.1, f32[16,2,128]{2,1,0:T(2,128)S(1)} %mul.165), kind=kLoop, calls=%fused_computation.1 | loop fusion | flops 2617344 | bytes 4276224 | tf_op jit(solution)/shard_map/reduce_sum | solution.py:47
  11.7 0.0 copy-start.9
  11.7 0.0 copy-start.8
  11.7 0.1 fusion.27
  11.8 0.1 copy.73
  11.9 0.1 broadcast_multiply_fusion
  12.0 0.0 copy-done.6
  12.0 1.2 %convolution_convert_fusion.2 = bf16[16,1024]{1,0:T(8,128)(2,1)S(1)} fusion(bf16[256,1024]{1,0:T(8,128)(2,1)} %param.23, f32[2,8,2,128]{3,2,1,0:T(2,128)S(1)} %bitcast.43, f32[256]{0:T(256)S(1)} %bitcast.47), kind=kOutput, calls=%fused_computation.10 | convolution fusion | flops 8413184 | bytes 574464 | tf_op jit(solution)/shard_map/dot_general | solution.py:53
  13.2 10.0 %psum.7 = bf16[16,1024]{1,0:T(8,128)(2,1)S(1)} all-reduce(bf16[16,1024]{1,0:T(8,128)(2,1)S(1)} %convolution_convert_fusion.2), channel_id=1, replica_groups=mesh['ep'=16,'tp'=2] {'tp'}, use_global_device_ids=true, to_apply=%region_3.4 | all-reduce | flops 16384 | bytes 65536 | tf_op jit(solution)/shard_map/psum | solution.py:54
  23.2 0.0 copy-done.3
  23.2 0.1 fusion.17
  23.3 0.0 copy-done.5
  23.3 0.3 convolution_convert_fusion
  23.6 0.9 %reshape.168 = bf16[16,12,1024]{2,1,0:T(8,128)(2,1)} reshape(bf16[192,1024]{1,0:T(8,128)(2,1)S(1)} %convolution_convert_fusion) | data formatting | bytes 786432 | tf_op jit(solution)/shard_map/reshape | solution.py:89
  24.5 5.9 %all-to-all-start = ((bf16[16,12,1024]{2,1,0:T(8,128)(2,1)}), bf16[16,12,1024]{2,1,0:T(8,128)(2,1)S(1)}, u32[]{:S(2)}, u32[]{:S(2)}) async-start(bf16[16,12,1024]{2,1,0:T(8,128)(2,1)} %reshape.168), calls=%async_computation | async-start | bytes 1048576 | tf_op jit(solution)/shard_map/all_to_all | solution.py:91
  30.5 0.0 copy-done.9
  30.5 0.2 fusion.42
  30.7 0.1 copy.76
  30.8 0.0 copy-done.8
  30.8 0.2 convolution_exponential_fusion
  31.0 0.1 copy.74
  31.1 0.1 copy.75
  31.1 13.6 %all-to-all-done = bf16[16,12,1024]{2,1,0:T(8,128)(2,1)S(1)} async-done(((bf16[16,12,1024]{2,1,0:T(8,128)(2,1)}), bf16[16,12,1024]{2,1,0:T(8,128)(2,1)S(1)}, u32[]{:S(2)}, u32[]{:S(2)}) %all-to-all-start) | async-done | bytes 393248 | tf_op jit(solution)/shard_map/all_to_all | solution.py:91
  44.7 0.1 reshape.169
  44.8 0.0 copy-done
  44.8 0.4 fusion.11
  45.2 0.0 copy-done.7
  45.2 0.0 copy-start.2
  45.2 0.4 fusion.1
  45.6 0.0 copy-start.4
  45.6 7.6 %all-gather = bf16[192,1024]{1,0:T(8,128)(2,1)S(1)} all-gather(bf16[192,512]{1,0:T(8,128)(2,1)S(1)} %fusion.1), channel_id=2, replica_groups=mesh['ep'=16,'tp'=2] {'tp'}, dimensions={1}, use_global_device_ids=true | all-gather | bytes 589824 | tf_op jit(solution)/shard_map/all_gather | solution.py:99
  53.2 0.0 copy-done.2
  53.2 0.4 fusion.2
  53.6 0.3 copy.92
  53.9 0.5 broadcast.119
  54.4 1.8 %reduce.1 = bf16[192,512]{1,0:T(8,128)(2,1)S(1)} reduce(bf16[192,1,512]{2,1,0:T(2,128)(2,1)S(1)} %bitcast.41, bf16[]{:T(256)} %broadcast.119), dimensions={1}, to_apply=%bitcast.40.reduce_sub_computation | reduce | bytes 393218
  56.3 0.8 %reshape.179 = bf16[16,2,3072]{2,1,0:T(2,128)(2,1)} reshape(bf16[192,512]{1,0:T(8,128)(2,1)S(1)} %reduce.1) | data formatting | bytes 393216
  57.0 4.4 %all-to-all-start.1 = ((bf16[16,2,3072]{2,1,0:T(2,128)(2,1)}), bf16[16,2,3072]{2,1,0:T(2,128)(2,1)S(1)}, u32[]{:S(2)}, u32[]{:S(2)}) async-start(bf16[16,2,3072]{2,1,0:T(2,128)(2,1)} %reshape.179), calls=%async_computation.1 | async-start | bytes 393216 | tf_op jit(solution)/shard_map/all_to_all | solution.py:103
  61.5 0.0 copy-done.4
  61.5 0.2 select_reduce_fusion
  61.7 8.7 %all-to-all-done.1 = bf16[16,2,3072]{2,1,0:T(2,128)(2,1)S(1)} async-done(((bf16[16,2,3072]{2,1,0:T(2,128)(2,1)}), bf16[16,2,3072]{2,1,0:T(2,128)(2,1)S(1)}, u32[]{:S(2)}, u32[]{:S(2)}) %all-to-all-start.1) | async-done | bytes 196640 | tf_op jit(solution)/shard_map/all_to_all | solution.py:103
  70.4 0.1 reshape.180
  70.5 0.2 fusion.3
  70.8 0.6 add_convert_fusion
  (13 shorter events, 0.1 us)
Async XLA Ops:
  0.6 44.2 %copy-start = (bf16[1,1024,512]{2,1,0:T(8,128)(2,1)S(1)}, bf16[1,1024,512]{2,1,0:T(8,128)(2,1)}, u32[]{:S(2)}) copy-start(bf16[1,1024,512]{2,1,0:T(8,128)(2,1)} %param.29) | copy-start | bytes 3145732
  0.6 8.0 %copy-start.1 = (f32[16,2,128,128]{3,2,1,0:T(8,128)S(1)}, f32[16,2,128,128]{3,2,1,0:T(8,128)}, u32[]{:S(2)}) copy-start(f32[16,2,128,128]{3,2,1,0:T(8,128)} %param.17) | copy-start | bytes 6291460
  8.6 3.4 %copy-start.6 = (f32[2,128]{1,0:T(2,128)S(1)}, f32[2,128]{1,0:T(2,128)}, u32[]{:S(2)}) copy-start(f32[2,128]{1,0:T(2,128)} %param.22) | copy-start | bytes 3076
  8.6 14.5 %copy-start.3 = (bf16[16,1024]{1,0:T(8,128)(2,1)S(1)}, bf16[16,1024]{1,0:T(8,128)(2,1)}, u32[]{:S(2)}) copy-start(bf16[16,1024]{1,0:T(8,128)(2,1)} %param.16) | copy-start | bytes 98308
  8.7 14.7 %copy-start.5 = (f32[1024]{0:T(1024)S(1)}, f32[1024]{0:T(1024)}, u32[]{:S(2)}) copy-start(f32[1024]{0:T(1024)} %param.25) | copy-start | bytes 12292
  11.7 18.8 %copy-start.9 = (bf16[1024,4]{0,1:T(4,128)(2,1)S(1)}, bf16[1024,4]{0,1:T(4,128)(2,1)}, u32[]{:S(2)}) copy-start(bf16[1024,4]{0,1:T(4,128)(2,1)} %param.26) | copy-start | bytes 24580
  11.7 19.1 %copy-start.8 = (bf16[1024,16]{0,1:T(8,128)(2,1)S(1)}, bf16[1024,16]{0,1:T(8,128)(2,1)}, u32[]{:S(2)}) copy-start(bf16[1024,16]{0,1:T(8,128)(2,1)} %param.27) | copy-start | bytes 98308
  24.5 20.7 %copy-start.7 = (bf16[1,1024,512]{2,1,0:T(8,128)(2,1)S(1)}, bf16[1,1024,512]{2,1,0:T(8,128)(2,1)}, u32[]{:S(2)}) copy-start(bf16[1,1024,512]{2,1,0:T(8,128)(2,1)} %param.30) | copy-start | bytes 3145732
  24.5 20.2 %all-to-all-start = ((bf16[16,12,1024]{2,1,0:T(8,128)(2,1)}), bf16[16,12,1024]{2,1,0:T(8,128)(2,1)S(1)}, u32[]{:S(2)}, u32[]{:S(2)}) async-start(bf16[16,12,1024]{2,1,0:T(8,128)(2,1)} %reshape.168), calls=%async_computation | async-start | bytes 1048576 | tf_op jit(solution)/shard_map/all_to_all | solution.py:91
  45.2 8.0 %copy-start.2 = (bf16[1,1024,512]{2,1,0:T(8,128)(2,1)S(1)}, bf16[1,1024,512]{2,1,0:T(8,128)(2,1)}, u32[]{:S(2)}) copy-start(bf16[1,1024,512]{2,1,0:T(8,128)(2,1)} %param.31) | copy-start | bytes 3145732
  45.6 15.8 %copy-start.4 = (s32[16,6]{0,1:T(8,128)S(1)}, s32[16,6]{0,1:T(8,128)}, u32[]{:S(2)}) copy-start(s32[16,6]{0,1:T(8,128)} %param.28) | copy-start | bytes 1156
  57.0 13.4 %all-to-all-start.1 = ((bf16[16,2,3072]{2,1,0:T(2,128)(2,1)}), bf16[16,2,3072]{2,1,0:T(2,128)(2,1)S(1)}, u32[]{:S(2)}, u32[]{:S(2)}) async-start(bf16[16,2,3072]{2,1,0:T(2,128)(2,1)} %reshape.179), calls=%async_computation.1 | async-start | bytes 393216 | tf_op jit(solution)/shard_map/all_to_all | solution.py:103
where the time goes:
time: 71.9 us; the launch traced here: 71.4 us
  waiting for transfers between devices  22.3 us (31%)
  blocking collectives  17.6 us (24%)
  starting transfers between devices  10.3 us (14%)
  other arithmetic  8.77 us (12%)
  matrix products  7.21 us (10%)
  local copies, waits for them, and re-layouts  4.28 us (6%)
  between operations  0.95 us (1%)
    all_to_all x1, waiting for transfers between devices, local(): lax.all_to_all(outgoing, 'ep', split_axis=0, concat_axis=1, tiled=True)  13.6 us
    psum x1, blocking collectives, local(): mixed = lax.psum(head_part.astype(jnp.bfloat16), 'tp')  9.95 us
    all_to_all x1, waiting for transfers between devices, local(): lax.all_to_all(produced, 'ep', split_axis=1, concat_axis=0, tiled=True)  8.72 us
    all_gather x1, blocking collectives, local(): lax.all_gather(hidden, 'tp', axis=2, tiled=True)  7.6 us
    all_to_all x1, starting transfers between devices, local(): lax.all_to_all(outgoing, 'ep', split_axis=0, concat_axis=1, tiled=True)  5.92 us
    all_to_all x1, starting transfers between devices, local(): lax.all_to_all(produced, 'ep', split_axis=1, concat_axis=0, tiled=True)  4.41 us
    reduce_sum x1, other arithmetic, local(): readout = jnp.sum(new_state * query[..., None], axis=2)  3.02 us
    unnamed x24, local copies, waits for them, and re-layouts  2.4 us
  transfers between devices with their start and end apart: 2, of which 2 were waited for; matrix products, arithmetic and copies ran while one was open for 1% of the time, Pallas kernels for 0%

commit v1 on v0

--- a/solution.py
+++ b/solution.py
@@ -88,7 +88,10 @@
         .astype(jnp.bfloat16)
         .reshape(experts, capacity, model_width)
     )
-    arrived = lax.all_to_all(outgoing, "ep", split_axis=0, concat_axis=1, tiled=True)
+    size = lax.axis_size("ep")
+    pieces = jnp.stack(jnp.split(outgoing, size, axis=0), axis=0)
+    pieces = lax.all_to_all(pieces, "ep", split_axis=0, concat_axis=0)
+    arrived = jnp.concatenate(pieces, axis=1)
     gate_hidden = jnp.einsum(
         "erd,edf->erf", arrived, gate_weight, preferred_element_type=jnp.float32
     )

time: 71.9 us -> 80.7 us (1.12)
  local copies, waits for them, and re-layouts: 4.28 us -> 13.1 us
    unnamed x24 -> x39, local copies, waits for them, and re-layouts: 2.4 us -> 11.5 us
    reshape x1 -> x0, local copies, waits for them, and re-layouts: 0.88 us -> none  [local(): outgoing = jnp.dot(spread, ffn_in, preferred_element_type=jnp.float32).as...]
where the time goes in v1:
time: 80.7 us; the launch traced here: 80.1 us
  waiting for transfers between devices  22.3 us (28%)
  blocking collectives  17.6 us (22%)
  local copies, waits for them, and re-layouts  13.1 us (16%)
  starting transfers between devices  10.2 us (13%)
  other arithmetic  8.77 us (11%)
  matrix products  7.2 us (9%)
  between operations  0.96 us (1%)
    all_to_all x1, waiting for transfers between devices, local(): pieces = lax.all_to_all(pieces, 'ep', split_axis=0, concat_axis=0)  13.6 us
    unnamed x39, local copies, waits for them, and re-layouts  11.5 us
    psum x1, blocking collectives, local(): mixed = lax.psum(head_part.astype(jnp.bfloat16), 'tp')  9.95 us
    all_to_all x1, waiting for transfers between devices, local(): lax.all_to_all(produced, 'ep', split_axis=1, concat_axis=0, tiled=True)  8.72 us
    all_gather x1, blocking collectives, local(): lax.all_gather(hidden, 'tp', axis=2, tiled=True)  7.62 us
    all_to_all x1, starting transfers between devices, local(): pieces = lax.all_to_all(pieces, 'ep', split_axis=0, concat_axis=0)  5.79 us
    all_to_all x1, starting transfers between devices, local(): lax.all_to_all(produced, 'ep', split_axis=1, concat_axis=0, tiled=True)  4.41 us
    reduce_sum x1, other arithmetic, local(): readout = jnp.sum(new_state * query[..., None], axis=2)  3.02 us
  transfers between devices with their start and end apart: 2, of which 2 were waited for; matrix products, arithmetic and copies ran while one was open for 1% of the time, Pallas kernels for 0%

profile of v1, /device:TPU:0, one launch (start us, length us, event | category | flops | bytes accessed | tf_op | source)
XLA Modules:
  0.0 80.1 jit_solution(11627043963104435541)
XLA Ops:
  0.6 0.0 copy-start
  0.7 0.9 %copy.77 = s32[16,6]{1,0:T(8,128)S(1)} copy(s32[16,6]{0,1:T(8,128)} %param.28) | data formatting | bytes 768 | tf_op args[12]
  1.6 0.1 eq.73
  1.7 0.1 fusion.25
  1.8 0.1 reduce_window_sum.11
  1.9 0.2 select_reduce_fusion.2
  2.1 0.1 reduce_sum.110
  2.1 0.1 copy.78
  2.2 0.7 multiply_add_fusion.1
  2.9 0.1 convert_reduce_fusion
  3.0 0.9 %fusion.20 = f32[16]{0:T(128)S(1)} fusion(bf16[16,1024]{1,0:T(8,128)(2,1)} %param.16), kind=kLoop, calls=%fused_computation.37 | loop fusion | flops 49136 | bytes 32832 | tf_op jit(solution)/shard_map/reduce_sum | solution.py:10
  3.9 1.3 %divide_multiply_fusion = f32[16,256]{1,0:T(8,128)S(1)} fusion(bf16[1024,256]{1,0:T(8,128)(2,1)} %param.18, bf16[16,1024]{1,0:T(8,128)(2,1)} %param.16, f32[1024]{0:T(1024)} %param.24, f32[16]{0:T(128)S(1)} %add_rsqrt_fusion.2), kind=kOutput, calls=%fused_computation.85 | convolution fusion | flops 8470528 | bytes 577600 | tf_op jit(solution)/shard_map/dot_general | solution.py:38
  5.3 1.3 %fusion.33 = f32[16,256]{1,0:T(8,128)S(1)} fusion(bf16[1024,256]{1,0:T(8,128)(2,1)} %param.20, bf16[16,1024]{1,0:T(8,128)(2,1)} %param.16, f32[1024]{0:T(1024)} %param.24, f32[16]{0:T(128)S(1)} %add_rsqrt_fusion.2), kind=kOutput, calls=%fused_computation.99 | convolution fusion | flops 8454144 | bytes 577600 | tf_op jit(solution)/shard_map/dot_general | solution.py:40
  6.6 0.7 broadcast_subtract_fusion.1
  7.3 1.3 %fusion.8 = f32[16,256]{1,0:T(8,128)S(1)} fusion(bf16[1024,256]{1,0:T(8,128)(2,1)} %param.19, f32[256]{0:T(256)S(1)} %broadcast_subtract_fusion.1, f32[256]{0:T(256)} %param.21, bf16[16,1024]{1,0:T(8,128)(2,1)} %param.16, f32[1024]{0:T(1024)} %param.24, f32[16]{0:T(128)S(1)} %add_rsqrt_fusion.2), kind=kOutput, calls=%fused_computation.16 | convolution fusion | flops 8474624 | bytes 579648 | tf_op jit(solution)/shard_map/dot_general | solution.py:39
  8.6 0.0 copy-start.3
  8.7 0.0 copy-start.5
  8.7 3.0 %multiply_reduce_fusion = (f32[16,2,128]{2,1,0:T(2,128)S(1)}, f32[16,2,128,128]{3,2,1,0:T(8,128)}) fusion(f32[16,2,128]{2,1,0:T(2,128)S(1)} %mul.173, f32[16,2,128]{2,1,0:T(2,128)S(1)} %mul.169, f32[16,2,128]{2,1,0:T(2,128)S(1)} %broadcast_subtract_fusion, f32[16,2,128,128]{3,2,1,0:T(8,128)S(1)} %copy-done.1, f32[16,2,128]{2,1,0:T(2,128)S(1)} %mul.165), kind=kLoop, calls=%fused_computation.1 | loop fusion | flops 2617344 | bytes 4276224 | tf_op jit(solution)/shard_map/reduce_sum | solution.py:47
  11.7 0.1 fusion.27
  11.8 0.1 copy.73
  11.9 0.1 broadcast_multiply_fusion
  12.0 1.2 %convolution_convert_fusion.2 = bf16[16,1024]{1,0:T(8,128)(2,1)S(1)} fusion(bf16[256,1024]{1,0:T(8,128)(2,1)} %param.23, f32[2,8,2,128]{3,2,1,0:T(2,128)S(1)} %bitcast.107, f32[256]{0:T(256)S(1)} %bitcast.111), kind=kOutput, calls=%fused_computation.10 | convolution fusion | flops 8413184 | bytes 574464 | tf_op jit(solution)/shard_map/dot_general | solution.py:53
  13.2 10.0 %psum.7 = bf16[16,1024]{1,0:T(8,128)(2,1)S(1)} all-reduce(bf16[16,1024]{1,0:T(8,128)(2,1)S(1)} %convolution_convert_fusion.2), channel_id=1, replica_groups=mesh['ep'=16,'tp'=2] {'tp'}, use_global_device_ids=true, to_apply=%region_3.4 | all-reduce | flops 16384 | bytes 65536 | tf_op jit(solution)/shard_map/psum | solution.py:54
  23.2 0.1 fusion.17
  23.3 0.3 convolution_convert_fusion
  23.6 0.6 constant_dynamic-update-slice_fusion.15
  24.2 0.6 constant_dynamic-update-slice_fusion.14
  24.9 0.6 constant_dynamic-update-slice_fusion.13
  25.5 0.6 constant_dynamic-update-slice_fusion.12
  26.1 0.6 constant_dynamic-update-slice_fusion.11
  26.7 0.6 constant_dynamic-update-slice_fusion.10
  27.3 0.6 constant_dynamic-update-slice_fusion.9
  27.9 0.6 constant_dynamic-update-slice_fusion.8
  28.5 0.6 constant_dynamic-update-slice_fusion.7
  29.1 0.6 constant_dynamic-update-slice_fusion.6
  29.7 0.6 constant_dynamic-update-slice_fusion.5
  30.3 0.6 constant_dynamic-update-slice_fusion.4
  31.0 0.6 constant_dynamic-update-slice_fusion.3
  31.6 0.6 constant_dynamic-update-slice_fusion.2
  32.2 0.6 constant_dynamic-update-slice_fusion.1
  32.8 0.6 constant_dynamic-update-slice_fusion
  33.4 5.8 %all-to-all-start = ((bf16[16,1,12,1024]{3,2,1,0:T(8,128)(2,1)}), bf16[16,1,12,1024]{3,2,1,0:T(8,128)(2,1)S(1)}, u32[]{:S(2)}, u32[]{:S(2)}) async-start(bf16[16,1,12,1024]{3,2,1,0:T(8,128)(2,1)} %constant_dynamic-update-slice_fusion), calls=%async_computation | async-start | bytes 1048576 | tf_op jit(solution)/shard_map/all_to_all | solution.py:93
  39.2 0.2 fusion.42
  39.4 0.1 copy.76
  39.5 0.2 convolution_exponential_fusion
  39.7 0.1 copy.74
  39.8 0.1 copy.75
  39.9 13.6 %all-to-all-done = bf16[16,1,12,1024]{3,2,1,0:T(8,128)(2,1)S(1)} async-done(((bf16[16,1,12,1024]{3,2,1,0:T(8,128)(2,1)}), bf16[16,1,12,1024]{3,2,1,0:T(8,128)(2,1)S(1)}, u32[]{:S(2)}, u32[]{:S(2)}) %all-to-all-start) | async-done | bytes 393248 | tf_op jit(solution)/shard_map/all_to_all | solution.py:93
  53.5 0.1 reshape.196
  53.6 0.4 fusion.11
  54.0 0.4 fusion.1
  54.4 0.0 copy-start.4
  54.4 7.6 %all-gather = bf16[192,1024]{1,0:T(8,128)(2,1)S(1)} all-gather(bf16[192,512]{1,0:T(8,128)(2,1)S(1)} %fusion.1), channel_id=2, replica_groups=mesh['ep'=16,'tp'=2] {'tp'}, dimensions={1}, use_global_device_ids=true | all-gather | bytes 589824 | tf_op jit(solution)/shard_map/all_gather | solution.py:102
  62.0 0.4 fusion.2
  62.4 0.3 copy.92
  62.7 0.5 broadcast.119
  63.2 1.8 %reduce.1 = bf16[192,512]{1,0:T(8,128)(2,1)S(1)} reduce(bf16[192,1,512]{2,1,0:T(2,128)(2,1)S(1)} %bitcast.105, bf16[]{:T(256)} %broadcast.119), dimensions={1}, to_apply=%bitcast.104.reduce_sub_computation | reduce | bytes 393218
  65.0 0.8 reshape.206
  65.8 4.4 %all-to-all-start.1 = ((bf16[16,2,3072]{2,1,0:T(2,128)(2,1)}), bf16[16,2,3072]{2,1,0:T(2,128)(2,1)S(1)}, u32[]{:S(2)}, u32[]{:S(2)}) async-start(bf16[16,2,3072]{2,1,0:T(2,128)(2,1)} %reshape.206), calls=%async_computation.1 | async-start | bytes 393216 | tf_op jit(solution)/shard_map/all_to_all | solution.py:106
  70.2 0.2 select_reduce_fusion
  70.4 8.7 %all-to-all-done.1 = bf16[16,2,3072]{2,1,0:T(2,128)(2,1)S(1)} async-done(((bf16[16,2,3072]{2,1,0:T(2,128)(2,1)}), bf16[16,2,3072]{2,1,0:T(2,128)(2,1)S(1)}, u32[]{:S(2)}, u32[]{:S(2)}) %all-to-all-start.1) | async-done | bytes 196640 | tf_op jit(solution)/shard_map/all_to_all | solution.py:106
  79.2 0.1 reshape.207
  79.3 0.2 fusion.3
  79.5 0.6 add_convert_fusion
  (28 shorter events, 0.2 us)
Async XLA Ops:
  0.6 52.9 %copy-start = (bf16[1,1024,512]{2,1,0:T(8,128)(2,1)S(1)}, bf16[1,1024,512]{2,1,0:T(8,128)(2,1)}, u32[]{:S(2)}) copy-start(bf16[1,1024,512]{2,1,0:T(8,128)(2,1)} %param.29) | copy-start | bytes 3145732
  0.6 8.0 %copy-start.1 = (f32[16,2,128,128]{3,2,1,0:T(8,128)S(1)}, f32[16,2,128,128]{3,2,1,0:T(8,128)}, u32[]{:S(2)}) copy-start(f32[16,2,128,128]{3,2,1,0:T(8,128)} %param.17) | copy-start | bytes 6291460
  8.6 3.4 %copy-start.6 = (f32[2,128]{1,0:T(2,128)S(1)}, f32[2,128]{1,0:T(2,128)}, u32[]{:S(2)}) copy-start(f32[2,128]{1,0:T(2,128)} %param.22) | copy-start | bytes 3076
  8.6 14.5 %copy-start.3 = (bf16[16,1024]{1,0:T(8,128)(2,1)S(1)}, bf16[16,1024]{1,0:T(8,128)(2,1)}, u32[]{:S(2)}) copy-start(bf16[16,1024]{1,0:T(8,128)(2,1)} %param.16) | copy-start | bytes 98308
  8.7 14.7 %copy-start.5 = (f32[1024]{0:T(1024)S(1)}, f32[1024]{0:T(1024)}, u32[]{:S(2)}) copy-start(f32[1024]{0:T(1024)} %param.25) | copy-start | bytes 12292
  11.7 27.5 %copy-start.9 = (bf16[1024,4]{0,1:T(4,128)(2,1)S(1)}, bf16[1024,4]{0,1:T(4,128)(2,1)}, u32[]{:S(2)}) copy-start(bf16[1024,4]{0,1:T(4,128)(2,1)} %param.26) | copy-start | bytes 24580
  11.7 27.8 %copy-start.8 = (bf16[1024,16]{0,1:T(8,128)(2,1)S(1)}, bf16[1024,16]{0,1:T(8,128)(2,1)}, u32[]{:S(2)}) copy-start(bf16[1024,16]{0,1:T(8,128)(2,1)} %param.27) | copy-start | bytes 98308
  32.2 21.8 %copy-start.7 = (bf16[1,1024,512]{2,1,0:T(8,128)(2,1)S(1)}, bf16[1,1024,512]{2,1,0:T(8,128)(2,1)}, u32[]{:S(2)}) copy-start(bf16[1,1024,512]{2,1,0:T(8,128)(2,1)} %param.30) | copy-start | bytes 3145732
  33.4 20.1 %all-to-all-start = ((bf16[16,1,12,1024]{3,2,1,0:T(8,128)(2,1)}), bf16[16,1,12,1024]{3,2,1,0:T(8,128)(2,1)S(1)}, u32[]{:S(2)}, u32[]{:S(2)}) async-start(bf16[16,1,12,1024]{3,2,1,0:T(8,128)(2,1)} %constant_dynamic-update-slice_fusion), calls=%async_computation | async-start | bytes 1048576 | tf_op jit(solution)/shard_map/all_to_all | solution.py:93
  54.0 8.0 %copy-start.2 = (bf16[1,1024,512]{2,1,0:T(8,128)(2,1)S(1)}, bf16[1,1024,512]{2,1,0:T(8,128)(2,1)}, u32[]{:S(2)}) copy-start(bf16[1,1024,512]{2,1,0:T(8,128)(2,1)} %param.31) | copy-start | bytes 3145732
  54.4 15.9 %copy-start.4 = (s32[16,6]{0,1:T(8,128)S(1)}, s32[16,6]{0,1:T(8,128)}, u32[]{:S(2)}) copy-start(s32[16,6]{0,1:T(8,128)} %param.28) | copy-start | bytes 1156
  65.8 13.4 %all-to-all-start.1 = ((bf16[16,2,3072]{2,1,0:T(2,128)(2,1)}), bf16[16,2,3072]{2,1,0:T(2,128)(2,1)S(1)}, u32[]{:S(2)}, u32[]{:S(2)}) async-start(bf16[16,2,3072]{2,1,0:T(2,128)(2,1)} %reshape.206), calls=%async_computation.1 | async-start | bytes 393216 | tf_op jit(solution)/shard_map/all_to_all | solution.py:106
